TPU v7x, 32 devices: a whole 2x2x4 slice. The times are simulated.
32 devices in a mesh: sp: 8 (over z, y), tp: 4 (over x, core).
Axes of the slice: x: 2, y: 2, z: 4, core: 2. Of those that a mesh axis runs over, the one named last changes fastest.
Arguments:
- skip_stream: bfloat16 [6144, 2048], P(('sp', 'tp')), may hold values from -24 to 24
- acceptance_signal: bfloat16 [6144, 2048], P('sp', 'tp'), may hold values from -6 to 6
- lookup_mapped: bfloat16 [6144, 2048], P('sp', 'tp'), may hold values from -12 to 12
- payload_mapped: bfloat16 [6144, 2048], P('sp', 'tp'), may hold values from -6 to 6
- result_switch: bfloat16 [6144, 2048], P('sp', 'tp'), may hold values from -6 to 6
- forget_dynamic_share: bfloat16 [6144, 2048], P('sp', 'tp'), may hold values from -4 to 4
- additive_forget_logarithm: float32 [6144, 32], P('sp', 'tp'), may hold values from -1 to 0
- forget_feature_offset: float32 [2048], P('tp'), may hold values from -11 to -3
- substitution_dynamic_share: bfloat16 [6144, 2048], P('sp', 'tp'), may hold values from -6 to 6
- substitution_feature_offset: float32 [2048], P('tp'), may hold values from -6.5 to 2.5
- diagonal_reward_scales: float32 [2048], P('tp'), may hold values from -0.9 to 0.9
- result_matrix: bfloat16 [2048, 2048], P('tp'), may hold values from -0.125 to 0.125
- mlp_rescaler: float32 [2048], replicated, may hold values from 0.1 to 1.9
- switch_matrix: bfloat16 [2048, 5120], P('sp', 'tp'), may hold values from -0.125 to 0.125
- expand_matrix: bfloat16 [2048, 5120], P('sp', 'tp'), may hold values from -0.125 to 0.125
- contract_matrix: bfloat16 [2048, 5120], P('sp', 'tp'), may hold values from -0.25 to 0.25
Outputs:
- mixed_out: bfloat16 [6144, 2048], P(('sp', 'tp'))
All inputs are finite; a program needn't handle non-finite values.
Results may differ from a plain program's by a relative error of at most 0.015.
Values may be sent and summed in bfloat16 or wider, within the bound.
A program may use at most 128 MiB of HBM per device.

v0:
```python
import functools

import jax
import jax.numpy as jnp
from jax import lax
from jax.experimental import pallas as pl
from jax.experimental.pallas import tpu as pltpu
from jax.sharding import PartitionSpec as P

PER_GROUP_DIMS = 64


norm_eps = 1e-06
group_eps = 0.00064
half_step = 0.5
exact = lax.Precision.HIGHEST

PAIR = 2 * PER_GROUP_DIMS
CHUNK = 64
ROWS_OUT = 256
NT = (((1,), (1,)), ((), ()))
NN = (((1,), (0,)), ((), ()))
TN = (((0,), (0,)), ((), ()))
bf16 = jnp.bfloat16
f32 = jnp.float32
P_SCORE, P_INV, P_SOLVE, P_OUT, P_STATE = 3, 1, 3, 3, 1


def mm(left, right, dims, passes):
    if passes == 6:
        return lax.dot_general(left, right, dims, precision=exact, preferred_element_type=f32)
    left_hi, right_hi = left.astype(bf16), right.astype(bf16)
    total = lax.dot_general(left_hi, right_hi, dims, preferred_element_type=f32)
    if passes == 3:
        left_lo = (left - left_hi.astype(f32)).astype(bf16)
        right_lo = (right - right_hi.astype(f32)).astype(bf16)
        total += lax.dot_general(left_hi, right_lo, dims, preferred_element_type=f32)
        total += lax.dot_general(left_lo, right_hi, dims, preferred_element_type=f32)
    return total


def halves(shape):
    return lax.broadcasted_iota(jnp.int32, shape, 1) < PER_GROUP_DIMS


def stack(values):
    first = halves(values.shape)
    zero = jnp.zeros_like(values)
    return jnp.concatenate([jnp.where(first, values, zero), jnp.where(first, zero, values)], 0)


def fold(values):
    size = values.shape[0] // 2
    return values[:size] + values[size:]


def head_sums(values):
    row = lax.broadcasted_iota(jnp.int32, (PAIR, PAIR), 0) // PER_GROUP_DIMS
    col = lax.broadcasted_iota(jnp.int32, (PAIR, PAIR), 1) // PER_GROUP_DIMS
    ones = jnp.where(row == col, 1.0, 0.0).astype(bf16)
    hi = values.astype(bf16)
    left = values - hi.astype(f32)
    mid = left.astype(bf16)
    low = (left - mid.astype(f32)).astype(bf16)
    return (
        jnp.dot(hi, ones, preferred_element_type=f32)
        + jnp.dot(mid, ones, preferred_element_type=f32)
        + jnp.dot(low, ones, preferred_element_type=f32)
    )


def recur_kernel(
    read_ref, key_ref, value_ref, forget_ref, added_ref, rate_ref, forget_off_ref, rate_off_ref,
    out_ref, coef_ref, state_out_ref, map_out_ref, memory,
):
    pairs = read_ref.shape[1] // PAIR
    span = range(pairs)
    row = lax.broadcasted_iota(jnp.int32, (PAIR, PAIR), 0)
    col = lax.broadcasted_iota(jnp.int32, (PAIR, PAIR), 1)
    diagonal = jnp.where(row == col, 1.0, 0.0)
    same_head = (row // CHUNK) == (col // CHUNK)
    strict = same_head & (col < row)
    inclusive = same_head & (col <= row)

    @pl.when(pl.program_id(0) == 0)
    def _():
        for p in span:
            memory[p, :PAIR] = jnp.zeros((PAIR, PAIR), f32)
            memory[p, PAIR:] = diagonal

    lower = (
        lax.broadcasted_iota(jnp.int32, (CHUNK, CHUNK), 1)
        <= lax.broadcasted_iota(jnp.int32, (CHUNK, CHUNK), 0)
    )
    lower = jnp.where(lower, 1.0, 0.0)
    first = halves((CHUNK, PAIR))
    at = [slice(p * PAIR, (p + 1) * PAIR) for p in span]
    decay_rate = [
        jax.nn.sigmoid(forget_off_ref[:, at[p]] + forget_ref[:, at[p]].astype(f32)) for p in span
    ]
    log_step = [
        -0.6065306597126334 * decay_rate[p]
        + jnp.where(first, added_ref[:, 2 * p : 2 * p + 1], added_ref[:, 2 * p + 1 : 2 * p + 2])
        for p in span
    ]
    cumulate = [mm(lower, log_step[p], NN, 6) for p in span]
    key = [key_ref[:, at[p]].astype(f32) for p in span]
    unit = [key[p] * lax.rsqrt(head_sums(key[p] * key[p]) + norm_eps) for p in span]
    erase = [
        unit[p] * jax.nn.sigmoid(rate_off_ref[:, at[p]] + rate_ref[:, at[p]].astype(f32))
        for p in span
    ]
    middle = [cumulate[p][CHUNK // 2 - 1 : CHUNK // 2] for p in span]
    last = [cumulate[p][CHUNK - 1 : CHUNK] for p in span]
    growth = [jnp.exp(cumulate[p] - middle[p]) for p in span]
    shrink = [jnp.exp(middle[p] - cumulate[p]) for p in span]
    to_middle = [jnp.exp(middle[p]) for p in span]
    from_middle = [jnp.exp(last[p] - middle[p]) for p in span]
    over_chunk = [jnp.exp(last[p]) for p in span]
    before = [jnp.exp(cumulate[p] - log_step[p] - middle[p]) * unit[p] for p in span]
    read = [read_ref[:, at[p]].astype(f32) * growth[p] for p in span]
    key_back = [key[p] * shrink[p] for p in span]
    erase_back = [erase[p] * shrink[p] for p in span]
    score = [
        mm(
            jnp.concatenate([stack(before[p]), stack(read[p])], 0),
            jnp.concatenate([stack(key_back[p]), stack(erase_back[p])], 0),
            NT,
            P_SCORE,
        )
        for p in span
    ]
    key_past = [jnp.where(strict, score[p][:PAIR, :PAIR], 0.0) for p in span]
    erase_past = [jnp.where(strict, score[p][:PAIR, PAIR:], 0.0) for p in span]
    key_read = [jnp.where(inclusive, score[p][PAIR:, :PAIR], 0.0) for p in span]
    erase_read = [jnp.where(inclusive, score[p][PAIR:, PAIR:], 0.0) for p in span]
    value = [stack(value_ref[:, at[p]]).astype(f32) for p in span]
    recall = [mm(key_past[p], value[p], NN, P_SOLVE) for p in span]
    inverse = [
        diagonal - jnp.where((row // 2) == (col // 2), erase_past[p], 0.0) for p in span
    ]
    size = 2
    while size < CHUNK:
        off = ((row // (2 * size)) == (col // (2 * size))) & ((row // size) != (col // size))
        part = [mm(jnp.where(off, erase_past[p], 0.0), inverse[p], NN, P_INV) for p in span]
        inverse = [inverse[p] - mm(inverse[p], part[p], NN, P_INV) for p in span]
        size *= 2
    solved = [
        mm(
            inverse[p],
            jnp.concatenate([recall[p], stack(before[p] * to_middle[p])], 1),
            NN,
            P_SOLVE,
        )
        for p in span
    ]
    inner = [
        mm(
            jnp.concatenate([key_read[p], -erase_read[p]], 1),
            jnp.concatenate(
                [jnp.concatenate([value[p], jnp.zeros_like(value[p])], 1), solved[p]], 0
            ),
            NN,
            P_OUT,
        )
        for p in span
    ]
    local = [fold(inner[p][:, :PAIR]) for p in span]
    from_start = [fold(inner[p][:, PAIR:]) + read[p] * to_middle[p] for p in span]
    both = [memory[p] for p in span]
    passed = [mm(from_start[p], both[p], NT, P_STATE) for p in span]
    for p in span:
        out_ref[:, at[p]] = local[p] + passed[p][:, :PAIR]
        coef_ref[:, at[p]] = passed[p][:, PAIR:].astype(bf16)
    key_end = [key_back[p] * from_middle[p] for p in span]
    erase_end = [erase_back[p] * from_middle[p] for p in span]
    recalled = [fold(solved[p][:, :PAIR]) for p in span]
    carried_map = [fold(solved[p][:, PAIR:]) for p in span]
    added = [
        mm(
            jnp.concatenate([value_ref[:, at[p]].astype(f32), -recalled[p]], 0),
            jnp.concatenate([key_end[p], erase_end[p]], 0),
            TN,
            P_OUT,
        )
        for p in span
    ]
    step_map = [mm(carried_map[p], erase_end[p], TN, P_OUT) for p in span]
    for p in span:
        moved = mm(both[p], jnp.where(same_head, step_map[p], 0.0), NN, P_STATE)
        kept = both[p] * over_chunk[p] - moved
        memory[p, :PAIR] = kept[:PAIR] + jnp.where(same_head, added[p], 0.0)
        memory[p, PAIR:] = kept[PAIR:]

    @pl.when(pl.program_id(0) == pl.num_programs(0) - 1)
    def _():
        for p in span:
            state_out_ref[p] = fold(memory[p, :PAIR]).astype(bf16)
            map_out_ref[p] = fold(memory[p, PAIR:]).astype(bf16)


def recurrence(read, key, value, forget, added, rate, forget_off, rate_off):
    length, breadth = read.shape
    pairs = breadth // PAIR
    wide = pl.BlockSpec((CHUNK, breadth), lambda c: (c, 0))
    vector = pl.BlockSpec((1, breadth), lambda c: (0, 0))
    closing = pl.BlockSpec((pairs, PER_GROUP_DIMS, PAIR), lambda c: (0, 0, 0))
    closing_shape = jax.ShapeDtypeStruct((pairs, PER_GROUP_DIMS, PAIR), bf16)
    return pl.pallas_call(
        recur_kernel,
        grid=(length // CHUNK,),
        in_specs=[
            wide, wide, wide, wide,
            pl.BlockSpec((CHUNK, added.shape[1]), lambda c: (c, 0)),
            wide, vector, vector,
        ],
        out_specs=[wide, wide, closing, closing],
        out_shape=[
            jax.ShapeDtypeStruct((length, breadth), f32),
            jax.ShapeDtypeStruct((length, breadth), bf16),
            closing_shape,
            closing_shape,
        ],
        scratch_shapes=[pltpu.VMEM((pairs, 2 * PAIR, PAIR), f32)],
        cost_estimate=pl.CostEstimate(
            flops=length * breadth * 200000, bytes_accessed=length * breadth * 16, transcendentals=0
        ),
        name="recurrence",
    )(read, key, value, forget, added, rate, forget_off[None, :], rate_off[None, :])


def share_kernel(mine_ref, all_ref, own_sem, send_sem, recv_sem):
    me, n = lax.axis_index("sp"), all_ref.shape[0]
    barrier = pltpu.get_barrier_semaphore()
    for step in range(1, n):
        pl.semaphore_signal(
            barrier,
            inc=1,
            device_id={"sp": lax.rem(me + step, n)},
            device_id_type=pl.DeviceIdType.MESH,
        )
    pl.semaphore_wait(barrier, n - 1)
    copies = [
        pltpu.make_async_remote_copy(
            src_ref=mine_ref,
            dst_ref=all_ref.at[me],
            send_sem=send_sem.at[step - 1],
            recv_sem=recv_sem.at[step - 1],
            device_id={"sp": lax.rem(me + step, n)},
            device_id_type=pl.DeviceIdType.MESH,
        )
        for step in range(1, n)
    ]
    for copy in copies:
        copy.start()
    own = pltpu.make_async_copy(mine_ref, all_ref.at[me], own_sem)
    own.start()
    own.wait()
    for copy in copies:
        copy.wait()


def share(mine):
    n = lax.axis_size("sp")
    everyone = pl.pallas_call(
        share_kernel,
        in_specs=[pl.BlockSpec(memory_space=pltpu.VMEM)],
        out_specs=pl.BlockSpec(memory_space=pltpu.VMEM),
        out_shape=jax.ShapeDtypeStruct((n,) + mine.shape, mine.dtype),
        scratch_shapes=[
            pltpu.SemaphoreType.DMA,
            pltpu.SemaphoreType.DMA((n - 1,)),
            pltpu.SemaphoreType.DMA((n - 1,)),
        ],
        compiler_params=pltpu.CompilerParams(collective_id=0, has_side_effects=True),
        cost_estimate=pl.CostEstimate(flops=0, bytes_accessed=40000000, transcendentals=0),
        name="share",
    )(mine)
    return everyone[:, 0], everyone[:, 1]


def merge_kernel(
    place_ref, local_ref, coef_ref, states_ref, maps_ref, read_ref, key_ref, value_ref,
    switch_ref, scales_ref, matrix_ref, out_ref, carried, merged,
):
    pairs = local_ref.shape[1] // PAIR
    span = range(pairs)

    @pl.when(pl.program_id(0) == 0)
    def _():
        for p in span:
            carried[p] = jnp.zeros((PAIR, PAIR), f32)

        def one(turn, _):
            for p in span:
                carried[p] = mm(
                    carried[p], stack(maps_ref[turn, p].astype(f32)), NN, 3
                ) + stack(states_ref[turn, p].astype(f32))
            return 0

        lax.fori_loop(0, place_ref[0], one, 0)

    for p in span:
        at = slice(p * PAIR, (p + 1) * PAIR)
        outcome = local_ref[:, at] + mm(coef_ref[:, at].astype(f32), carried[p], NT, 1)
        centred = outcome - head_sums(outcome) * (1.0 / PER_GROUP_DIMS)
        spread = head_sums(centred * centred) * (1.0 / PER_GROUP_DIMS)
        normed = centred * lax.rsqrt(spread + group_eps)
        reward = head_sums(
            read_ref[:, at].astype(f32) * key_ref[:, at].astype(f32) * scales_ref[:, at]
        )
        merged[:, at] = (
            (normed + reward * value_ref[:, at].astype(f32)) * switch_ref[:, at].astype(f32)
        ).astype(bf16)
    out_ref[...] = jnp.dot(merged[...], matrix_ref[...], preferred_element_type=f32).astype(bf16)


def merge(place, local, coef, states, maps, read, key, value, switch, scales, matrix):
    length, breadth = local.shape
    pairs = breadth // PAIR
    rows = ROWS_OUT if length % ROWS_OUT == 0 else CHUNK
    wide = pl.BlockSpec((rows, breadth), lambda c: (c, 0))
    whole = pl.BlockSpec(states.shape, lambda c: (0, 0, 0, 0))
    return pl.pallas_call(
        merge_kernel,
        grid=(length // rows,),
        in_specs=[
            pl.BlockSpec(memory_space=pltpu.SMEM),
            wide, wide, whole, whole, wide, wide, wide, wide,
            pl.BlockSpec((1, breadth), lambda c: (0, 0)),
            pl.BlockSpec(matrix.shape, lambda c: (0, 0)),
        ],
        out_specs=pl.BlockSpec((rows, matrix.shape[1]), lambda c: (c, 0)),
        out_shape=jax.ShapeDtypeStruct((length, matrix.shape[1]), bf16),
        scratch_shapes=[pltpu.VMEM((pairs, PAIR, PAIR), f32), pltpu.VMEM((rows, breadth), bf16)],
        cost_estimate=pl.CostEstimate(
            flops=2 * length * breadth * matrix.shape[1],
            bytes_accessed=length * breadth * 14 + 2 * matrix.size + 2 * length * matrix.shape[1],
            transcendentals=0,
        ),
        name="merge",
    )(place, local, coef, states, maps, read, key, value, switch, scales[None, :], matrix)


def per_device(
    skip_stream,
    acceptance_signal,
    lookup_mapped,
    payload_mapped,
    result_switch,
    forget_dynamic_share,
    additive_forget_logarithm,
    forget_feature_offset,
    substitution_dynamic_share,
    substitution_feature_offset,
    diagonal_reward_scales,
    result_matrix,
    mlp_rescaler,
    switch_matrix,
    expand_matrix,
    contract_matrix,
):
    gate_whole, up_whole, down_whole = (
        lax.all_gather(switch_matrix, "sp", axis=0, tiled=True),
        lax.all_gather(expand_matrix, "sp", axis=0, tiled=True),
        lax.all_gather(contract_matrix, "sp", axis=0, tiled=True),
    )
    local, coef, state, move = recurrence(
        acceptance_signal,
        lookup_mapped,
        payload_mapped,
        forget_dynamic_share,
        additive_forget_logarithm,
        substitution_dynamic_share,
        forget_feature_offset,
        substitution_feature_offset,
    )
    states, maps = share(jnp.stack([state, move]))
    local, gate_whole = lax.optimization_barrier((local, gate_whole))
    partial_rows = merge(
        lax.axis_index("sp").astype(jnp.int32)[None],
        local,
        coef,
        states,
        maps,
        acceptance_signal,
        lookup_mapped,
        payload_mapped,
        result_switch,
        diagonal_reward_scales,
        result_matrix,
    )
    projected = lax.psum_scatter(
        partial_rows,
        "tp",
        scatter_dimension=0,
        tiled=True,
    )
    stream = skip_stream.astype(jnp.float32) + lax.optimization_barrier(projected).astype(
        jnp.float32
    )
    scale_rows = lax.rsqrt(jnp.mean(stream * stream, axis=-1, keepdims=True) + norm_eps)
    normed_rows = (stream * scale_rows * mlp_rescaler[None, :]).astype(jnp.bfloat16)
    normed_rows, up_whole = lax.optimization_barrier((normed_rows, up_whole))
    whole_rows = lax.all_gather(normed_rows, "tp", axis=0, tiled=True)
    gate_act = jnp.dot(whole_rows, gate_whole, preferred_element_type=jnp.float32)
    up_act = jnp.dot(whole_rows, up_whole, preferred_element_type=jnp.float32)
    hidden = (jax.nn.silu(gate_act) * up_act).astype(jnp.bfloat16)
    row_block = hidden
    ffn_out = lax.psum_scatter(
        lax.dot_general(
            row_block, down_whole, (((1,), (1,)), ((), ())), preferred_element_type=jnp.float32
        ).astype(jnp.bfloat16),
        "tp",
        scatter_dimension=0,
        tiled=True,
    )
    return (stream + half_step * lax.optimization_barrier(ffn_out).astype(jnp.float32)).astype(
        jnp.bfloat16
    )


def solution(mesh):
    placed = (
        P(("sp", "tp"), None),
        P("sp", "tp"),
        P("sp", "tp"),
        P("sp", "tp"),
        P("sp", "tp"),
        P("sp", "tp"),
        P("sp", "tp"),
        P("tp"),
        P("sp", "tp"),
        P("tp"),
        P("tp"),
        P("tp", None),
        P(),
        P("sp", "tp"),
        P("sp", "tp"),
        P("sp", "tp"),
    )
    return jax.shard_map(
        per_device, mesh=mesh, in_specs=placed, out_specs=P(("sp", "tp"), None), check_vma=False
    )
```

profile of v0, /device:TPU:0, one launch (start us, length us, event | category | flops | bytes accessed | tf_op | source)
XLA Modules:
  0.0 434.5 jit_solution(16075991706849202710)
XLA Ops:
  6.5 0.0 all-gather.5.cloned.1.call-start
  6.5 0.7 all-gather.5.cloned.1.call-update
  7.3 0.0 reduce-scatter.3.cloned.1.call-start
  7.3 1.7 copy.17.added_ref
  9.0 45.7 %recurrence.1 = (f32[768,512]{1,0:T(8,128)}, bf16[768,512]{1,0:T(8,128)(2,1)}, bf16[4,64,128]{2,1,0:T(8,128)(2,1)}, bf16[4,64,128]{2,1,0:T(8,128)(2,1)}) custom-call(bf16[768,512]{1,0:T(8,128)(2,1)} %read_ref.3, bf16[768,512]{1,0:T(8,128)(2,1)} %key_ref.3, bf16[768,512]{1,0:T(8,128)(2,1)} %value_ref.3, bf16[768,512]{1,0:T(8,128)(2,1)} %forget_ref.1, ...), custom_call_target="tpu_custom_call" | custom-call | flops 78643200000 | bytes 6291456 | tf_op jit(solution)/shard_map/recurrence/pallas_call | solution.py:209
  54.7 1.5 pad_maximum_fusion.mine_ref
  56.2 42.5 %share.1 = bf16[8,2,4,64,128]{4,3,2,1,0:T(8,128)(2,1)} custom-call(bf16[2,4,64,128]{3,2,1,0:T(8,128)(2,1)} %pad_maximum_fusion.mine_ref), custom_call_target="tpu_custom_call" | custom-call | bytes 40000000 | tf_op jit(solution)/shard_map/share/pallas_call | solution.py:265
  98.7 2.4 slice_bitcast_fusion
  101.0 17.5 %all-gather.5.cloned.1.call-done = bf16[2048,1280]{1,0:T(8,128)(2,1)} async-done(((bf16[256,1280]{1,0:T(8,128)(2,1)}), bf16[2048,1280]{1,0:T(8,128)(2,1)}) %all-gather.5.cloned.1.call-update) | async-done | bytes 5242896 | tf_op jit(solution)/shard_map/all_gather | solution.py:364
  118.5 11.3 %merge.1 = bf16[768,2048]{1,0:T(8,128)(2,1)} custom-call(s32[1]{0:T(128)} %bitcast.place_ref, f32[768,512]{1,0:T(8,128)} %get-tuple-element.14.local_ref, bf16[768,512]{1,0:T(8,128)(2,1)} %get-tuple-element.15.coef_ref, bf16[8,4,64,128]{3,2,1,0:T(8,128)(2,1)} %get-tuple-element.22.states_ref, bf16[8,4,64,128]{3,2,1,0:T(8,128)(2,1)} %get-tuple-element.21.maps_ref, ...), custom_call_target="tpu_custom_call" | custom-call | flops 1610612736 | bytes 10747904 | tf_op jit(solution)/shard_map/merge/pallas_call | solution.py:324
  129.8 0.0 copy-start
  129.8 0.0 copy-start.2
  129.8 0.0 reduce-scatter.3.cloned.1.call-update
  129.9 0.0 all-gather.7.cloned.1.call-start
  129.9 0.7 all-gather.7.cloned.1.call-update
  130.6 0.0 all-gather.9.cloned.1.call-start
  130.6 38.2 %reduce-scatter.3.cloned.1.call-done = bf16[192,2048]{1,0:T(8,128)(2,1)} async-done(((bf16[768,2048]{1,0:T(8,128)(2,1)}), bf16[192,2048]{1,0:T(8,128)(2,1)}) %reduce-scatter.3.cloned.1.call-update) | async-done | bytes 786448 | tf_op jit(solution)/shard_map/reduce_scatter | solution.py:393
  168.8 0.0 copy-done
  168.8 1.5 multiply_reduce_fusion
  170.3 0.0 copy-done.2
  170.3 2.3 multiply_convert_fusion
  172.6 84.3 %all-gather.7.cloned.1.call-done = bf16[2048,1280]{1,0:T(8,128)(2,1)} async-done(((bf16[256,1280]{1,0:T(8,128)(2,1)}), bf16[2048,1280]{1,0:T(8,128)(2,1)}) %all-gather.7.cloned.1.call-update) | async-done | bytes 5242896 | tf_op jit(solution)/shard_map/all_gather | solution.py:365
  257.0 0.0 all-gather.9.cloned.1.call-update
  257.0 0.0 all-gather.11.cloned.1.call-start
  257.0 0.5 all-gather.11.cloned.1.call-update
  257.6 0.2 reduce-scatter.5.cloned.1.call-start
  257.8 27.3 %all-gather.9.cloned.1.call-done = bf16[768,2048]{1,0:T(8,128)(2,1)} async-done(((bf16[192,2048]{1,0:T(8,128)(2,1)}), bf16[768,2048]{1,0:T(8,128)(2,1)}) %all-gather.9.cloned.1.call-update) | async-done | bytes 3145744 | tf_op jit(solution)/shard_map/all_gather | solution.py:405
  285.1 9.6 %fusion.2 = f32[768,1280]{1,0:T(8,128)} fusion(bf16[768,2048]{1,0:T(8,128)(2,1)} %all-gather.9.cloned.1.call-done, bf16[2048,1280]{1,0:T(8,128)(2,1)} %all-gather.5.cloned.1.call-done), kind=kOutput, calls=%fused_computation.12 | convolution fusion | flops 4026531840 | bytes 12320768 | tf_op jit(solution)/shard_map/dot_general | solution.py:406
  294.7 78.4 %all-gather.11.cloned.1.call-done = bf16[2048,1280]{1,0:T(8,128)(2,1)} async-done(((bf16[256,1280]{1,0:T(8,128)(2,1)}), bf16[2048,1280]{1,0:T(8,128)(2,1)}) %all-gather.11.cloned.1.call-update) | async-done | bytes 5242896 | tf_op jit(solution)/shard_map/all_gather | solution.py:366
  373.1 16.0 %convolution_convert_fusion = bf16[768,2048]{1,0:T(8,128)(2,1)} fusion(bf16[2048,1280]{1,0:T(8,128)(2,1)} %all-gather.11.cloned.1.call-done, bf16[768,2048]{1,0:T(8,128)(2,1)} %all-gather.9.cloned.1.call-done, bf16[2048,1280]{1,0:T(8,128)(2,1)} %all-gather.7.cloned.1.call-done, f32[768,1280]{1,0:T(8,128)} %fusion.2), kind=kOutput, calls=%fused_computation.2 | convolution fusion | flops 8060534784 | bytes 20709376 | tf_op jit(solution)/shard_map/dot_general | solution.py:411
  389.0 0.0 copy-start.1
  389.0 0.0 reduce-scatter.5.cloned.1.call-update
  389.0 36.2 %reduce-scatter.5.cloned.1.call-done = bf16[192,2048]{1,0:T(8,128)(2,1)} async-done(((bf16[768,2048]{1,0:T(8,128)(2,1)}), bf16[192,2048]{1,0:T(8,128)(2,1)}) %reduce-scatter.5.cloned.1.call-update) | async-done | bytes 786448 | tf_op jit(solution)/shard_map/reduce_scatter | solution.py:410
  425.3 0.0 copy-done.1
  425.3 2.4 add_convert_fusion
  (1 shorter events, 0.0 us)
Async XLA Ops:
  6.5 112.0 %all-gather.5.cloned.1.call-start = ((), (), s32[]{:S(2)}) async-start(), calls=%async_computation.2 | async-start | bytes 5898240 | tf_op jit(solution)/shard_map/all_gather | solution.py:364
  7.3 161.6 %reduce-scatter.3.cloned.1.call-start = ((), (), s32[]{:S(2)}) async-start(), calls=%async_computation.3 | async-start | bytes 3932160 | tf_op jit(solution)/shard_map/reduce_scatter | solution.py:393
  129.8 39.0 %copy-start = (bf16[192,2048]{1,0:T(8,128)(2,1)S(1)}, bf16[192,2048]{1,0:T(8,128)(2,1)}, u32[]{:S(2)}) copy-start(bf16[192,2048]{1,0:T(8,128)(2,1)} %param.16) | copy-start | bytes 2359300
  129.8 40.5 %copy-start.2 = (f32[2048]{0:T(1024)S(1)}, f32[2048]{0:T(1024)}, u32[]{:S(2)}) copy-start(f32[2048]{0:T(1024)} %param.28) | copy-start | bytes 24580
  129.9 127.1 %all-gather.7.cloned.1.call-start = ((), (), s32[]{:S(2)}) async-start(), calls=%async_computation.4 | async-start | bytes 5898240 | tf_op jit(solution)/shard_map/all_gather | solution.py:365
  130.6 154.5 %all-gather.9.cloned.1.call-start = ((), (), s32[]{:S(2)}) async-start(), calls=%async_computation.5 | async-start | bytes 3932160 | tf_op jit(solution)/shard_map/all_gather | solution.py:405
  257.0 116.1 %all-gather.11.cloned.1.call-start = ((), (), s32[]{:S(2)}) async-start(), calls=%async_computation.6 | async-start | bytes 5898240 | tf_op jit(solution)/shard_map/all_gather | solution.py:366
  257.6 167.7 %reduce-scatter.5.cloned.1.call-start = ((), (), s32[]{:S(2)}) async-start(), calls=%async_computation.7 | async-start | bytes 3932160 | tf_op jit(solution)/shard_map/reduce_scatter | solution.py:410
  389.0 36.2 %copy-start.1 = (bf16[192,2048]{1,0:T(8,128)(2,1)S(1)}, bf16[192,2048]{1,0:T(8,128)(2,1)}, u32[]{:S(2)}) copy-start(bf16[192,2048]{1,0:T(8,128)(2,1)} %reduce-scatter.3.cloned.1.call-done) | copy-start | bytes 2359300
Sparse Core Ops, SparseCore 0:
  9.5 108.9 all-gather.4
  130.0 38.8 reduce-scatter.2
  171.0 85.8 all-gather.6
  258.4 26.6 all-gather.8
  287.1 85.8 all-gather.10
  389.2 36.0 reduce-scatter.4
where the time goes:
time: 435 us
  waiting for transfers between devices  284 us (65%)
  Pallas kernels  99.5 us (23%)
  matrix products  25.5 us (6%)
  between operations  13.5 us (3%)
  other arithmetic  7.74 us (2%)
    all_gather x1, waiting for transfers between devices, per_device(): lax.all_gather(expand_matrix, 'sp', axis=0, tiled=True)  84.3 us
    all_gather x1, waiting for transfers between devices, per_device(): lax.all_gather(contract_matrix, 'sp', axis=0, tiled=True)  78.4 us
    pallas_call x1, Pallas kernels, recurrence(): pl.pallas_call(recur_kernel, grid=(length // CHUNK,), in_specs=[wide, wid...  45.7 us
    pallas_call x1, Pallas kernels, share(): pl.pallas_call(share_kernel, in_specs=[pl.BlockSpec(memory_space=pltpu.VM...  42.5 us
    reduce_scatter x1, waiting for transfers between devices, per_device(): lax.psum_scatter(partial_rows, 'tp', scatter_dimension=0, tiled=True)  38.2 us
    reduce_scatter x1, waiting for transfers between devices, per_device(): lax.psum_scatter(lax.dot_general(row_block, down_whole, (((1,), (1,)), ((...  36.2 us
    all_gather x1, waiting for transfers between devices, per_device(): whole_rows = lax.all_gather(normed_rows, 'tp', axis=0, tiled=True)  27.3 us
    all_gather x1, waiting for transfers between devices, per_device(): lax.all_gather(switch_matrix, 'sp', axis=0, tiled=True)  17.5 us
  transfers between devices with their start and end apart: 6, of which 6 were waited for; matrix products, arithmetic and copies ran while one was open for 4% of the time, Pallas kernels for 20%

commit v1 on v0

v1 whole, which is shorter than its diff:
```python
import functools

import jax
import jax.numpy as jnp
from jax import lax
from jax.experimental import pallas as pl
from jax.experimental.pallas import tpu as pltpu
from jax.sharding import PartitionSpec as P

PER_GROUP_DIMS = 64


norm_eps = 1e-06
group_eps = 0.00064
half_step = 0.5
exact = lax.Precision.HIGHEST

PAIR = 2 * PER_GROUP_DIMS
CHUNK = 64
ROWS_OUT = 256
NT = (((1,), (1,)), ((), ()))
NN = (((1,), (0,)), ((), ()))
TN = (((0,), (0,)), ((), ()))
bf16 = jnp.bfloat16
f32 = jnp.float32
P_SCORE, P_INV, P_SOLVE, P_OUT, P_STATE = 3, 1, 3, 3, 1


def mm(left, right, dims, passes):
    if passes == 6:
        return lax.dot_general(left, right, dims, precision=exact, preferred_element_type=f32)
    left_hi, right_hi = left.astype(bf16), right.astype(bf16)
    total = lax.dot_general(left_hi, right_hi, dims, preferred_element_type=f32)
    if passes == 3:
        left_lo = (left - left_hi.astype(f32)).astype(bf16)
        right_lo = (right - right_hi.astype(f32)).astype(bf16)
        total += lax.dot_general(left_hi, right_lo, dims, preferred_element_type=f32)
        total += lax.dot_general(left_lo, right_hi, dims, preferred_element_type=f32)
    return total


def halves(shape):
    return lax.broadcasted_iota(jnp.int32, shape, 1) < PER_GROUP_DIMS


def stack(values):
    first = halves(values.shape)
    zero = jnp.zeros_like(values)
    return jnp.concatenate([jnp.where(first, values, zero), jnp.where(first, zero, values)], 0)


def fold(values):
    size = values.shape[0] // 2
    return values[:size] + values[size:]


def head_sums(values):
    row = lax.broadcasted_iota(jnp.int32, (PAIR, PAIR), 0) // PER_GROUP_DIMS
    col = lax.broadcasted_iota(jnp.int32, (PAIR, PAIR), 1) // PER_GROUP_DIMS
    ones = jnp.where(row == col, 1.0, 0.0).astype(bf16)
    hi = values.astype(bf16)
    left = values - hi.astype(f32)
    mid = left.astype(bf16)
    low = (left - mid.astype(f32)).astype(bf16)
    return (
        jnp.dot(hi, ones, preferred_element_type=f32)
        + jnp.dot(mid, ones, preferred_element_type=f32)
        + jnp.dot(low, ones, preferred_element_type=f32)
    )


def advance_chunk(
    here, read_ref, key_ref, value_ref, forget_ref, added_ref, rate_ref, forget_off_ref,
    rate_off_ref, local_ref, coef_ref, memory,
):
    pairs = read_ref.shape[1] // PAIR
    span = range(pairs)
    row = lax.broadcasted_iota(jnp.int32, (PAIR, PAIR), 0)
    col = lax.broadcasted_iota(jnp.int32, (PAIR, PAIR), 1)
    diagonal = jnp.where(row == col, 1.0, 0.0)
    same_head = (row // CHUNK) == (col // CHUNK)
    strict = same_head & (col < row)
    inclusive = same_head & (col <= row)

    lower = (
        lax.broadcasted_iota(jnp.int32, (CHUNK, CHUNK), 1)
        <= lax.broadcasted_iota(jnp.int32, (CHUNK, CHUNK), 0)
    )
    lower = jnp.where(lower, 1.0, 0.0)
    first = halves((CHUNK, PAIR))
    at = [slice(p * PAIR, (p + 1) * PAIR) for p in span]
    decay_rate = [
        jax.nn.sigmoid(forget_off_ref[:, at[p]] + forget_ref[here, at[p]].astype(f32)) for p in span
    ]
    log_step = [
        -0.6065306597126334 * decay_rate[p]
        + jnp.where(first, added_ref[here, 2 * p : 2 * p + 1], added_ref[here, 2 * p + 1 : 2 * p + 2])
        for p in span
    ]
    cumulate = [mm(lower, log_step[p], NN, 6) for p in span]
    key = [key_ref[here, at[p]].astype(f32) for p in span]
    unit = [key[p] * lax.rsqrt(head_sums(key[p] * key[p]) + norm_eps) for p in span]
    erase = [
        unit[p] * jax.nn.sigmoid(rate_off_ref[:, at[p]] + rate_ref[here, at[p]].astype(f32))
        for p in span
    ]
    middle = [cumulate[p][CHUNK // 2 - 1 : CHUNK // 2] for p in span]
    last = [cumulate[p][CHUNK - 1 : CHUNK] for p in span]
    growth = [jnp.exp(cumulate[p] - middle[p]) for p in span]
    shrink = [jnp.exp(middle[p] - cumulate[p]) for p in span]
    to_middle = [jnp.exp(middle[p]) for p in span]
    from_middle = [jnp.exp(last[p] - middle[p]) for p in span]
    over_chunk = [jnp.exp(last[p]) for p in span]
    before = [jnp.exp(cumulate[p] - log_step[p] - middle[p]) * unit[p] for p in span]
    read = [read_ref[here, at[p]].astype(f32) * growth[p] for p in span]
    key_back = [key[p] * shrink[p] for p in span]
    erase_back = [erase[p] * shrink[p] for p in span]
    score = [
        mm(
            jnp.concatenate([stack(before[p]), stack(read[p])], 0),
            jnp.concatenate([stack(key_back[p]), stack(erase_back[p])], 0),
            NT,
            P_SCORE,
        )
        for p in span
    ]
    key_past = [jnp.where(strict, score[p][:PAIR, :PAIR], 0.0) for p in span]
    erase_past = [jnp.where(strict, score[p][:PAIR, PAIR:], 0.0) for p in span]
    key_read = [jnp.where(inclusive, score[p][PAIR:, :PAIR], 0.0) for p in span]
    erase_read = [jnp.where(inclusive, score[p][PAIR:, PAIR:], 0.0) for p in span]
    value = [stack(value_ref[here, at[p]]).astype(f32) for p in span]
    recall = [mm(key_past[p], value[p], NN, P_SOLVE) for p in span]
    inverse = [
        diagonal - jnp.where((row // 2) == (col // 2), erase_past[p], 0.0) for p in span
    ]
    size = 2
    while size < CHUNK:
        off = ((row // (2 * size)) == (col // (2 * size))) & ((row // size) != (col // size))
        part = [mm(jnp.where(off, erase_past[p], 0.0), inverse[p], NN, P_INV) for p in span]
        inverse = [inverse[p] - mm(inverse[p], part[p], NN, P_INV) for p in span]
        size *= 2
    solved = [
        mm(
            inverse[p],
            jnp.concatenate([recall[p], stack(before[p] * to_middle[p])], 1),
            NN,
            P_SOLVE,
        )
        for p in span
    ]
    inner = [
        mm(
            jnp.concatenate([key_read[p], -erase_read[p]], 1),
            jnp.concatenate(
                [jnp.concatenate([value[p], jnp.zeros_like(value[p])], 1), solved[p]], 0
            ),
            NN,
            P_OUT,
        )
        for p in span
    ]
    local = [fold(inner[p][:, :PAIR]) for p in span]
    from_start = [fold(inner[p][:, PAIR:]) + read[p] * to_middle[p] for p in span]
    both = [memory[p] for p in span]
    passed = [mm(from_start[p], both[p], NT, P_STATE) for p in span]
    for p in span:
        local_ref[here, at[p]] = local[p] + passed[p][:, :PAIR]
        coef_ref[here, at[p]] = passed[p][:, PAIR:].astype(bf16)
    key_end = [key_back[p] * from_middle[p] for p in span]
    erase_end = [erase_back[p] * from_middle[p] for p in span]
    recalled = [fold(solved[p][:, :PAIR]) for p in span]
    carried_map = [fold(solved[p][:, PAIR:]) for p in span]
    added = [
        mm(
            jnp.concatenate([value_ref[here, at[p]].astype(f32), -recalled[p]], 0),
            jnp.concatenate([key_end[p], erase_end[p]], 0),
            TN,
            P_OUT,
        )
        for p in span
    ]
    step_map = [mm(carried_map[p], erase_end[p], TN, P_OUT) for p in span]
    for p in span:
        moved = mm(both[p], jnp.where(same_head, step_map[p], 0.0), NN, P_STATE)
        kept = both[p] * over_chunk[p] - moved
        memory[p, :PAIR] = kept[:PAIR] + jnp.where(same_head, added[p], 0.0)
        memory[p, PAIR:] = kept[PAIR:]


class Layout:
    def __init__(self, mesh):
        self.n_sp, self.n_tp = mesh.shape["sp"], mesh.shape["tp"]
        devices = list(mesh.devices.flat)
        spots = [getattr(d, "coords", None) for d in devices]
        self.lanes = self.cores = 1
        if all(s is not None for s in spots):
            self.lanes = len({s[1] for s in spots})
            self.cores = len({getattr(d, "core_on_chip", 0) for d in devices})
        if self.n_sp % self.lanes:
            self.lanes = 1
        if self.n_tp % self.cores:
            self.cores = 1
        self.planes, self.sides = self.n_sp // self.lanes, self.n_tp // self.cores


def to(**where):
    return dict(device_id=where, device_id_type=pl.DeviceIdType.MESH)


def chain(total, step):
    return mm(total, step, NN, 1) + mm(total - total.astype(bf16).astype(f32), step, NN, 1)


GATE, UP, DOWN = range(3)


class Relay:
    def __init__(self, lay, blocks, whole, send_sem, recv_sem, own_sem):
        self.lay, self.blocks, self.whole, self.own_sem = lay, blocks, whole, own_sem
        self.send_sem, self.recv_sem = send_sem, recv_sem
        me = lax.axis_index("sp")
        self.z, self.y = me // lay.lanes, lax.rem(me, lay.lanes)
        self.depth = blocks[0].shape[0]

    def slot(self, hop, lane):
        return (hop + self.lay.planes - 1) * self.lay.lanes + lane

    def held(self, hop):
        return (self.z >= hop) & (self.z < self.lay.planes + hop)

    def part(self, matrix, hop, lane):
        source = (self.z - hop) * self.lay.lanes + lax.rem(
            self.y + self.lay.lanes - lane, self.lay.lanes
        )
        first = pl.multiple_of(source * self.depth, self.depth)
        return self.whole.at[matrix, pl.ds(first, self.depth)]

    def copy(self, matrix, source, place, plane, lane):
        return pltpu.make_async_remote_copy(
            src_ref=self.blocks[matrix] if source == (0, 0) else self.part(matrix, *source),
            dst_ref=self.part(matrix, *source),
            send_sem=self.send_sem.at[matrix, self.slot(*place)],
            recv_sem=self.recv_sem.at[matrix, self.slot(*place)],
            **to(sp=plane * self.lay.lanes + lane),
        )

    def ahead(self, matrix, hop, way):
        there = self.z + way
        wanted = self.held(hop) & (there >= 0) & (there < self.lay.planes)
        return self.copy(matrix, (hop, 0), (hop + way, 0), there, self.y), wanted

    def aside(self, matrix, hop, lane):
        beside = lax.rem(self.y + lane, self.lay.lanes)
        return self.copy(matrix, (hop, 0), (hop, lane), self.z, beside), self.held(hop)

    def start(self, pair):
        pl.when(pair[1])(pair[0].start)

    def own(self, matrix):
        return pltpu.make_async_copy(
            self.blocks[matrix], self.part(matrix, 0, 0), self.own_sem.at[matrix]
        )

    def arrive(self, matrix, hop, lane):
        piece = self.part(matrix, hop, lane)
        slot = self.slot(hop, lane)
        wait = pltpu.make_async_remote_copy(
            src_ref=piece,
            dst_ref=piece,
            send_sem=self.send_sem.at[matrix, slot],
            recv_sem=self.recv_sem.at[matrix, slot],
            **to(sp=lax.axis_index("sp")),
        ).wait_recv
        pl.when(self.held(hop))(wait)

    def take(self, matrix, reach):
        for hop in (reach, -reach):
            self.arrive(matrix, hop, 0)

    def forward(self, matrix, reach):
        for way in (1, -1):
            self.start(self.ahead(matrix, way * reach, way))

    def cross(self, matrix, reach):
        for hop in (reach, -reach) if reach else (0,):
            for lane in range(1, self.lay.lanes):
                self.start(self.aside(matrix, hop, lane))

    def settle(self, matrix):
        last = self.lay.planes - 1
        for reach in range(last + 1):
            for way in (1, -1):
                if reach < last:
                    copy, wanted = self.ahead(matrix, way * reach, way)
                    pl.when(wanted)(copy.wait_send)
            for hop in (reach, -reach) if reach else (0,):
                for lane in range(1, self.lay.lanes):
                    copy, wanted = self.aside(matrix, hop, lane)
                    pl.when(wanted)(copy.wait_send)


def layer_kernel(lay, steps, *refs):
    (
        skip_ref, read_ref, key_ref, value_ref, switch_ref, forget_ref, added_ref, forget_off_ref,
        rate_ref, rate_off_ref, scales_ref, matrix_ref, gain_ref, gate_ref, up_ref, down_ref,
        out_ref,
        local_ref, coef_ref, memory, lane_ref, plane_ref, mine_ref, carried_ref, mixed, gathered,
        matrix, stream_ref, rows_ref, hidden_ref, whole, own, inner, near, outer, far,
        relay_send, relay_recv, own_sem, lane_send, lane_recv, plane_send, plane_recv,
        load_sem, matrix_send, matrix_recv, out_sem, in_sem, row_send, row_recv,
        near_send, near_recv, far_send, far_recv,
    ) = refs
    n = lay.n_tp
    rows, width = skip_ref.shape
    length, breadth = read_ref.shape
    pairs = breadth // PAIR
    span = range(pairs)
    last = lay.planes - 1
    spot, me = lax.axis_index("sp"), lax.axis_index("tp")
    z, y = spot // lay.lanes, lax.rem(spot, lay.lanes)
    x, c = me // lay.cores, lax.rem(me, lay.cores)
    beside = [z * lay.lanes + lax.rem(y + s, lay.lanes) for s in range(1, lay.lanes)]
    line = [lax.rem(spot + s * lay.lanes, lay.n_sp) for s in range(1, lay.planes)]
    peers = [lax.rem(me + s, n) for s in range(1, n)]
    partners = [x * lay.cores + lax.rem(c + j, lay.cores) for j in range(1, lay.cores)]
    remote = [lax.rem(x + i, lay.sides) * lay.cores + c for i in range(1, lay.sides)]

    barrier = pltpu.get_barrier_semaphore()
    for axis, others in (("sp", beside + line), ("tp", peers)):
        for other in others:
            pl.semaphore_signal(barrier, inc=1, **to(**{axis: other}))
    pl.semaphore_wait(barrier, len(beside) + len(line) + len(peers))

    relay = Relay(lay, (gate_ref, up_ref, down_ref), whole, relay_send, relay_recv, own_sem)
    for m in (GATE, UP):
        relay.forward(m, 0) if last else None
        relay.cross(m, 0)
    for m in (GATE, UP, DOWN):
        relay.own(m).start()

    def place_matrix(i, j):
        side, core = lax.rem(x + lay.sides - i, lay.sides), lax.rem(c + lay.cores - j, lay.cores)
        return side * lay.cores + core

    def pass_matrix(i, j):
        source = matrix_ref if i == 0 or j == 0 else matrix.at[i, 0]
        target = partners[j - 1] if j else remote[i - 1]
        return pltpu.make_async_remote_copy(
            src_ref=source,
            dst_ref=matrix.at[i, j],
            send_sem=matrix_send.at[i, j],
            recv_sem=matrix_recv.at[i, j],
            **to(tp=target),
        )

    own_matrix = pltpu.make_async_copy(matrix_ref, matrix.at[0, 0], load_sem)
    own_matrix.start()
    for i in range(1, lay.sides):
        pass_matrix(i, 0).start()
    for j in range(1, lay.cores):
        pass_matrix(0, j).start()

    diagonal = jnp.where(
        lax.broadcasted_iota(jnp.int32, (PAIR, PAIR), 0)
        == lax.broadcasted_iota(jnp.int32, (PAIR, PAIR), 1),
        1.0,
        0.0,
    )
    for p in span:
        memory[p, :PAIR] = jnp.zeros((PAIR, PAIR), f32)
        memory[p, PAIR:] = diagonal

    chunks = length // CHUNK

    def one(turn, _):
        if last:

            @pl.when(turn == chunks // 3)
            def _():
                relay.take(GATE, 1)
                if last > 1:
                    relay.forward(GATE, 1)
                for lane in range(1, lay.lanes):
                    relay.start(relay.aside(GATE, 1, lane))

            @pl.when(turn == 2 * chunks // 3)
            def _():
                relay.take(UP, 1)

        here = pl.ds(pl.multiple_of(turn * CHUNK, CHUNK), CHUNK)
        advance_chunk(
            here, read_ref, key_ref, value_ref, forget_ref, added_ref, rate_ref, forget_off_ref,
            rate_off_ref, local_ref, coef_ref, memory,
        )
        return 0

    lax.fori_loop(0, chunks, one, 0)

    for p in span:
        lane_ref[y, 0, p] = fold(memory[p, :PAIR]).astype(bf16)
        lane_ref[y, 1, p] = fold(memory[p, PAIR:]).astype(bf16)
    lane_copies = [
        pltpu.make_async_remote_copy(
            src_ref=lane_ref.at[y],
            dst_ref=lane_ref.at[y],
            send_sem=lane_send.at[s],
            recv_sem=lane_recv.at[s],
            **to(sp=other),
        )
        for s, other in enumerate(beside)
    ]
    for copy in lane_copies:
        copy.start()
    if last:
        for lane in range(1, lay.lanes):
            relay.start(relay.aside(GATE, -1, lane))
        relay.cross(UP, 1)
    for copy in lane_copies:
        copy.wait_recv()
    state = [stack(lane_ref[0, 0, p].astype(f32)) for p in span]
    move = [stack(lane_ref[0, 1, p].astype(f32)) for p in span]
    own_state = [jnp.where(y > 0, state[p], 0.0) for p in span]
    own_move = [jnp.where(y > 0, move[p], diagonal) for p in span]
    for t in range(1, lay.lanes):
        for p in span:
            step = stack(lane_ref[t, 1, p].astype(f32))
            state[p] = chain(state[p], step) + stack(lane_ref[t, 0, p].astype(f32))
            move[p] = chain(move[p], step)
            if t < lay.lanes - 1:
                own_state[p] = jnp.where(y > t, state[p], own_state[p])
                own_move[p] = jnp.where(y > t, move[p], own_move[p])
    for p in span:
        mine_ref[0, p] = fold(state[p]).astype(bf16)
        mine_ref[1, p] = fold(move[p]).astype(bf16)

    def onward(s):
        return pltpu.make_async_remote_copy(
            src_ref=mine_ref,
            dst_ref=plane_ref.at[s - 1],
            send_sem=plane_send.at[s - 1],
            recv_sem=plane_recv.at[s - 1],
            **to(sp=line[s - 1]),
        )

    for s in range(1, lay.planes):
        pl.when(z + s < lay.planes)(onward(s).start)
    if last > 1:
        relay.forward(UP, 1)
        relay.take(GATE, 2)
        if last > 2:
            relay.forward(GATE, 2)
        relay.cross(GATE, 2)
    for p in span:
        carried_ref[p] = jnp.zeros((PAIR, PAIR), f32)
    for s in range(last, 0, -1):

        @pl.when(z >= s)
        def _(s=s):
            onward(s).wait_recv()
            for p in span:
                carried_ref[p] = chain(
                    carried_ref[p], stack(plane_ref[s - 1, 1, p].astype(f32))
                ) + stack(plane_ref[s - 1, 0, p].astype(f32))

    for p in span:
        carried_ref[p] = chain(carried_ref[p], own_move[p]) + own_state[p]

    for i in range(1, lay.sides):
        pass_matrix(i, 0).wait_recv()
        for j in range(1, lay.cores):
            pass_matrix(i, j).start()

    def send(s):
        return pltpu.make_async_remote_copy(
            src_ref=mixed.at[s],
            dst_ref=gathered.at[s],
            send_sem=out_sem.at[s],
            recv_sem=in_sem.at[s],
            **to(tp=peers[s]),
        )

    for s in range(n):
        target = peers[s] if s < n - 1 else me
        here = pl.ds(pl.multiple_of(target * rows, rows), rows)
        for p in span:
            at = slice(p * PAIR, (p + 1) * PAIR)
            outcome = local_ref[here, at] + mm(coef_ref[here, at].astype(f32), carried_ref[p], NT, 1)
            centred = outcome - head_sums(outcome) * (1.0 / PER_GROUP_DIMS)
            spread = head_sums(centred * centred) * (1.0 / PER_GROUP_DIMS)
            normed = centred * lax.rsqrt(spread + group_eps)
            reward = head_sums(
                read_ref[here, at].astype(f32) * key_ref[here, at].astype(f32) * scales_ref[:, at]
            )
            block = (
                (normed + reward * value_ref[here, at].astype(f32))
                * switch_ref[here, at].astype(f32)
            ).astype(bf16)
            if s < n - 1:
                mixed[s, :, at] = block
            else:
                gathered[s, :, at] = block
        if s < n - 1:
            send(s).start()
    if last > 1:
        relay.take(UP, 2)
        if last > 2:
            relay.forward(UP, 2)
        relay.cross(UP, 2)
    for s in range(n - 1):
        send(s).wait_recv()
    own_matrix.wait()
    for i in range(lay.sides):
        for j in range(1, lay.cores):
            pass_matrix(i, j).wait_recv()
    total = jnp.zeros((rows, width), f32)
    for i in range(lay.sides):
        for j in range(lay.cores):
            slot = lax.rem(me - place_matrix(i, j) + 2 * n - 1, n)
            total += jnp.dot(gathered[slot], matrix[i, j], preferred_element_type=f32)
    stream = skip_ref[...].astype(f32) + total.astype(bf16).astype(f32)
    stream_ref[...] = stream
    scale = lax.rsqrt(jnp.mean(stream * stream, axis=-1, keepdims=True) + norm_eps)
    mine = pl.ds(pl.multiple_of(me * rows, rows), rows)
    rows_ref[mine] = (stream * scale * gain_ref[...]).astype(bf16)

    def pass_rows(source, target, slot):
        piece = rows_ref.at[pl.ds(pl.multiple_of(source * rows, rows), rows)]
        return pltpu.make_async_remote_copy(
            src_ref=piece,
            dst_ref=piece,
            send_sem=row_send.at[slot],
            recv_sem=row_recv.at[slot],
            **to(tp=target),
        )

    row_copies = []
    for i in range(1, lay.sides):
        copy = pass_rows(me, remote[i - 1], i * lay.cores)
        copy.start()
        row_copies.append(copy)
    for i in range(lay.sides):
        source = lax.rem(x + lay.sides - i, lay.sides) * lay.cores + c
        if i:
            row_copies[i - 1].wait_recv()
        for j in range(1, lay.cores):
            copy = pass_rows(source, partners[j - 1], i * lay.cores + j)
            copy.start()
            row_copies.append(copy)
    for r in range(3, last + 1):
        for m in (GATE, UP):
            relay.take(m, r)
            if r < last:
                relay.forward(m, r)
            relay.cross(m, r)
    if last:
        relay.forward(DOWN, 0)
    relay.cross(DOWN, 0)
    for copy in row_copies[lay.sides - 1 :]:
        copy.wait_recv()

    for m in (GATE, UP):
        relay.own(m).wait()
        for lane in range(1, lay.lanes):
            for hop in range(-last, last + 1):
                relay.arrive(m, hop, lane)

    def down_step(r):
        if r <= last:
            relay.take(DOWN, r)
            if r < last:
                relay.forward(DOWN, r)
            relay.cross(DOWN, r)

    down_step(1)
    units = hidden_ref.shape[1]
    tile = 256 if units % 256 == 0 else 128 if units % 128 == 0 else units
    for first in range(0, units, tile):
        columns = slice(first, first + tile)
        gated = jnp.dot(rows_ref[...], whole[GATE, :, columns], preferred_element_type=f32)
        raised = jnp.dot(rows_ref[...], whole[UP, :, columns], preferred_element_type=f32)
        hidden_ref[:, columns] = (gated * jax.nn.sigmoid(gated) * raised).astype(bf16)

    relay.own(DOWN).wait()
    part = width // lay.planes
    order = list(range(1, lay.sides)) + [0]
    hops = [0] + [way * r for r in range(1, last + 1) for way in (1, -1)]

    def within(t, i, j):
        return pltpu.make_async_remote_copy(
            src_ref=inner.at[t, j - 1, i],
            dst_ref=near.at[t, j - 1, i],
            send_sem=near_send.at[t, i, j - 1],
            recv_sem=near_recv.at[t, i, j - 1],
            **to(tp=partners[j - 1]),
        )

    def between(t, i):
        return pltpu.make_async_remote_copy(
            src_ref=outer.at[t, i - 1],
            dst_ref=far.at[t, i - 1],
            send_sem=far_send.at[t, i - 1],
            recv_sem=far_recv.at[t, i - 1],
            **to(tp=remote[i - 1]),
        )

    def product(weight, i, j):
        target = lax.rem(x + i, lay.sides) * lay.cores + lax.rem(c + j, lay.cores)
        piece = hidden_ref[pl.ds(pl.multiple_of(target * rows, rows), rows)]
        return lax.dot_general(piece, weight, NT, preferred_element_type=f32)

    for t, hop in enumerate(hops):
        if hop >= 0:
            down_step(hop + 2)
        for lane in range(1, lay.lanes):
            relay.arrive(DOWN, hop, lane)

        @pl.when(relay.held(hop))
        def _(t=t, hop=hop):
            weight = whole[DOWN, pl.ds(pl.multiple_of((z - hop) * part, part), part)]
            for i in order:
                for j in range(1, lay.cores):
                    inner[t, j - 1, i] = product(weight, i, j).astype(bf16)
                    within(t, i, j).start()
            for i in order:
                own[t, i] = product(weight, i, 0)
            for i in order:
                sums = own[t, i]
                for j in range(1, lay.cores):
                    within(t, i, j).wait_recv()
                    sums += near[t, j - 1, i].astype(f32)
                if i:
                    outer[t, i - 1] = sums.astype(bf16)
                    between(t, i).start()
                else:
                    own[t, 0] = sums

    for t, hop in enumerate(hops):

        @pl.when(relay.held(hop))
        def _(t=t, hop=hop):
            columns = pl.ds(pl.multiple_of((z - hop) * part, part), part)
            sums = own[t, 0]
            for i in range(1, lay.sides):
                between(t, i).wait_recv()
                sums += far[t, i - 1].astype(f32)
            sums = sums.astype(bf16).astype(f32)
            out_ref[:, columns] = (stream_ref[:, columns] + half_step * sums).astype(bf16)

    for m in (GATE, UP, DOWN):
        relay.settle(m)
    for copy in lane_copies + row_copies:
        copy.wait_send()
    for s in range(1, lay.planes):
        pl.when(z + s < lay.planes)(onward(s).wait_send)
    for i in range(lay.sides):
        for j in range(lay.cores):
            if i or j:
                pass_matrix(i, j).wait_send()
    for s in range(n - 1):
        send(s).wait_send()
    for t, hop in enumerate(hops):

        @pl.when(relay.held(hop))
        def _(t=t):
            for i in order:
                for j in range(1, lay.cores):
                    within(t, i, j).wait_send()
                if i:
                    between(t, i).wait_send()


def per_device(
    lay,
    skip_stream,
    acceptance_signal,
    lookup_mapped,
    payload_mapped,
    result_switch,
    forget_dynamic_share,
    additive_forget_logarithm,
    forget_feature_offset,
    substitution_dynamic_share,
    substitution_feature_offset,
    diagonal_reward_scales,
    result_matrix,
    mlp_rescaler,
    switch_matrix,
    expand_matrix,
    contract_matrix,
):
    rows, width = skip_stream.shape
    length, breadth = acceptance_signal.shape
    depth, units = switch_matrix.shape
    pairs = breadth // PAIR
    n = lay.n_tp
    one = (2, pairs, PER_GROUP_DIMS, PAIR)
    lanes, planes = max(lay.lanes - 1, 1), max(lay.planes - 1, 1)
    cores, sides = max(lay.cores - 1, 1), max(lay.sides - 1, 1)
    places = (2 * lay.planes - 1) * lay.lanes
    hops = 2 * lay.planes - 1
    part = width // lay.planes
    dma = pltpu.SemaphoreType.DMA
    vmem, anywhere = pl.BlockSpec(memory_space=pltpu.VMEM), pl.BlockSpec(memory_space=pl.ANY)
    return pl.pallas_call(
        functools.partial(layer_kernel, lay, hops),
        in_specs=[vmem] * 11 + [anywhere, vmem] + [anywhere] * 3,
        out_specs=vmem,
        out_shape=jax.ShapeDtypeStruct((rows, width), bf16),
        scratch_shapes=[
            pltpu.VMEM((length, breadth), f32),
            pltpu.VMEM((length, breadth), bf16),
            pltpu.VMEM((pairs, 2 * PAIR, PAIR), f32),
            pltpu.VMEM((lay.lanes,) + one, bf16),
            pltpu.VMEM((planes,) + one, bf16),
            pltpu.VMEM(one, bf16),
            pltpu.VMEM((pairs, PAIR, PAIR), f32),
            pltpu.VMEM((n - 1, rows, breadth), bf16),
            pltpu.VMEM((n, rows, breadth), bf16),
            pltpu.VMEM((lay.sides, lay.cores, breadth, width), bf16),
            pltpu.VMEM((rows, width), f32),
            pltpu.VMEM((length, width), bf16),
            pltpu.VMEM((length, units), bf16),
            pltpu.VMEM((3, width, units), bf16),
            pltpu.VMEM((hops, lay.sides, rows, part), f32),
            pltpu.VMEM((hops, cores, lay.sides, rows, part), bf16),
            pltpu.VMEM((hops, cores, lay.sides, rows, part), bf16),
            pltpu.VMEM((hops, sides, rows, part), bf16),
            pltpu.VMEM((hops, sides, rows, part), bf16),
            dma((3, places)),
            dma((3, places)),
            dma((3,)),
            dma((lanes,)),
            dma((lanes,)),
            dma((planes,)),
            dma((planes,)),
            dma,
            dma((lay.sides, lay.cores)),
            dma((lay.sides, lay.cores)),
            dma((n,)),
            dma((n,)),
            dma((n,)),
            dma((n,)),
            dma((hops, lay.sides, cores)),
            dma((hops, lay.sides, cores)),
            dma((hops, sides)),
            dma((hops, sides)),
        ],
        compiler_params=pltpu.CompilerParams(
            collective_id=0, has_side_effects=True, vmem_limit_bytes=63 * 2**20
        ),
        cost_estimate=pl.CostEstimate(
            flops=6 * length * width * units, bytes_accessed=6 * width * units, transcendentals=0
        ),
        name="layer",
    )(
        skip_stream,
        acceptance_signal,
        lookup_mapped,
        payload_mapped,
        result_switch,
        forget_dynamic_share,
        additive_forget_logarithm,
        forget_feature_offset[None, :],
        substitution_dynamic_share,
        substitution_feature_offset[None, :],
        diagonal_reward_scales[None, :],
        result_matrix,
        mlp_rescaler[None, :],
        switch_matrix,
        expand_matrix,
        contract_matrix,
    )


def solution(mesh):
    placed = (
        P(("sp", "tp"), None),
        P("sp", "tp"),
        P("sp", "tp"),
        P("sp", "tp"),
        P("sp", "tp"),
        P("sp", "tp"),
        P("sp", "tp"),
        P("tp"),
        P("sp", "tp"),
        P("tp"),
        P("tp"),
        P("tp", None),
        P(),
        P("sp", "tp"),
        P("sp", "tp"),
        P("sp", "tp"),
    )
    return jax.shard_map(
        functools.partial(per_device, Layout(mesh)),
        mesh=mesh,
        in_specs=placed,
        out_specs=P(("sp", "tp"), None),
        check_vma=False,
    )
```

time: 435 us -> 212 us (0.49)
  waiting for transfers between devices: 284 us -> 0 us
  Pallas kernels: 99.5 us -> 208 us
  matrix products: 25.5 us -> 0 us
  between operations: 13.5 us -> 0.01 us
  other arithmetic: 7.74 us -> 0 us
    all_gather x4 -> x0, waiting for transfers between devices: 207 us -> none  [the longest x1 84.3 us: per_device(): lax.all_gather(expand_matrix, 'sp', axis=0, tiled=True)]
    pallas_call x3 -> x1, Pallas kernels: 99.5 us -> 208 us  [per_device(): pl.pallas_call(functools.partial(layer_kernel, lay, hops), in_specs=[vmem...]
    reduce_scatter x2 -> x0, waiting for transfers between devices: 74.4 us -> none  [the longest x1 38.2 us: per_device(): lax.psum_scatter(partial_rows, 'tp', scatter_dimension=0, tiled=True)]
    dot_general x2 -> x0, matrix products: 25.5 us -> none  [the longest x1 16 us: per_device(): lax.dot_general(row_block, down_whole, (((1,), (1,)), ((), ())), preferre...]
    convert_element_type x2 -> x0, other arithmetic: 4.73 us -> none  [the longest x1 2.42 us: per_device(): (stream + half_step * lax.optimization_barrier(ffn_out).astype(jnp.float3...]
  transfers between devices with their start and end apart: 6 -> 0, of which waited for: 6 -> 0; matrix products, arithmetic and copies ran while one was open for 4% -> 0% of each run, Pallas kernels for 20% -> 0%
where the time goes in v1:
time: 212 us; the launch traced here: 211 us
  Pallas kernels  208 us (98%)
  local copies, waits for them, and re-layouts  3.74 us (2%)
    pallas_call x1, Pallas kernels, per_device(): pl.pallas_call(functools.partial(layer_kernel, lay, hops), in_specs=[vmem...  208 us

profile of v1, /device:TPU:0, one launch (start us, length us, event | category | flops | bytes accessed | tf_op | source)
XLA Modules:
  0.0 211.5 jit_solution(3857701151369057548)
XLA Ops:
  0.0 1.6 copy.17.refs_6_
  1.7 207.7 %layer.1 = bf16[192,2048]{1,0:T(8,128)(2,1)} custom-call(bf16[192,2048]{1,0:T(8,128)(2,1)} %refs_0_.1, bf16[768,512]{1,0:T(8,128)(2,1)} %refs_1_.1, bf16[768,512]{1,0:T(8,128)(2,1)} %refs_2_.1, bf16[768,512]{1,0:T(8,128)(2,1)} %refs_3_.1, bf16[768,512]{1,0:T(8,128)(2,1)} %refs_4_.1, bf16[768,512]{1,0:T(8,128)(2,1)} %refs_5_.1, f32[768,8]{1,0:T(8,128)} %copy.17.refs_6_, ...), custom_call_target="tpu_custom_call" | custom-call | flops 12079595520 | bytes 15728640 | tf_op jit(solution)/shard_map/layer/pallas_call | solution.py:704
  209.4 2.1 copy.19

commit v2 on v1

--- a/solution.py
+++ b/solution.py
@@ -212,6 +212,7 @@
 
 
 GATE, UP, DOWN = range(3)
+WIDE = (UP,)
 
 
 class Relay:
@@ -228,6 +229,12 @@
     def held(self, hop):
         return (self.z >= hop) & (self.z < self.lay.planes + hop)
 
+    def wide(self, matrix, hop):
+        if matrix not in WIDE:
+            return False
+        first, last = self.z == hop, self.z == self.lay.planes - 1 + hop
+        return first | last if hop == 0 else first if hop > 0 else last
+
     def part(self, matrix, hop, lane):
         source = (self.z - hop) * self.lay.lanes + lax.rem(
             self.y + self.lay.lanes - lane, self.lay.lanes
@@ -244,14 +251,19 @@
             **to(sp=plane * self.lay.lanes + lane),
         )
 
-    def ahead(self, matrix, hop, way):
+    def ahead(self, matrix, hop, way, lane=0):
         there = self.z + way
         wanted = self.held(hop) & (there >= 0) & (there < self.lay.planes)
-        return self.copy(matrix, (hop, 0), (hop + way, 0), there, self.y), wanted
+        if lane:
+            wanted = wanted & self.wide(matrix, hop)
+        return self.copy(matrix, (hop, lane), (hop + way, lane), there, self.y), wanted
 
     def aside(self, matrix, hop, lane):
         beside = lax.rem(self.y + lane, self.lay.lanes)
-        return self.copy(matrix, (hop, 0), (hop, lane), self.z, beside), self.held(hop)
+        wanted = self.held(hop)
+        if hop and matrix in WIDE:
+            wanted = wanted & ~self.wide(matrix, hop)
+        return self.copy(matrix, (hop, 0), (hop, lane), self.z, beside), wanted
 
     def start(self, pair):
         pl.when(pair[1])(pair[0].start)
@@ -261,7 +273,7 @@
             self.blocks[matrix], self.part(matrix, 0, 0), self.own_sem.at[matrix]
         )
 
-    def arrive(self, matrix, hop, lane):
+    def arrive(self, matrix, hop, lane, wide=None):
         piece = self.part(matrix, hop, lane)
         slot = self.slot(hop, lane)
         wait = pltpu.make_async_remote_copy(
@@ -271,7 +283,10 @@
             recv_sem=self.recv_sem.at[matrix, slot],
             **to(sp=lax.axis_index("sp")),
         ).wait_recv
-        pl.when(self.held(hop))(wait)
+        wanted = self.held(hop)
+        if wide is not None and matrix in WIDE:
+            wanted = wanted & (self.wide(matrix, hop) if wide else ~self.wide(matrix, hop))
+        pl.when(wanted)(wait)
 
     def take(self, matrix, reach):
         for hop in (reach, -reach):
@@ -280,6 +295,16 @@
     def forward(self, matrix, reach):
         for way in (1, -1):
             self.start(self.ahead(matrix, way * reach, way))
+
+    def take_wide(self, matrix, reach):
+        for hop in (reach, -reach):
+            for lane in range(1, self.lay.lanes):
+                self.arrive(matrix, hop, lane, wide=True)
+
+    def forward_wide(self, matrix, reach):
+        for way in (1, -1):
+            for lane in range(1, self.lay.lanes):
+                self.start(self.ahead(matrix, way * reach, way, lane))
 
     def cross(self, matrix, reach):
         for hop in (reach, -reach) if reach else (0,):
@@ -291,8 +316,9 @@
         for reach in range(last + 1):
             for way in (1, -1):
                 if reach < last:
-                    copy, wanted = self.ahead(matrix, way * reach, way)
-                    pl.when(wanted)(copy.wait_send)
+                    for lane in range(self.lay.lanes if matrix in WIDE else 1):
+                        copy, wanted = self.ahead(matrix, way * reach, way, lane)
+                        pl.when(wanted)(copy.wait_send)
             for hop in (reach, -reach) if reach else (0,):
                 for lane in range(1, self.lay.lanes):
                     copy, wanted = self.aside(matrix, hop, lane)
@@ -300,16 +326,19 @@
 
 
 def layer_kernel(lay, steps, *refs):
+    forget_off_ref, rate_off_ref, scales_ref, gain_ref, *given = refs[:16]
+    given, (matrix_ref, gate_ref, up_ref, down_ref) = given[:8], given[8:12]
+    out_ref = refs[16]
+    loaded = refs[17:25]
+    read_ref, key_ref, value_ref, forget_ref, added_ref, rate_ref, switch_ref, skip_ref = loaded
     (
-        skip_ref, read_ref, key_ref, value_ref, switch_ref, forget_ref, added_ref, forget_off_ref,
-        rate_ref, rate_off_ref, scales_ref, matrix_ref, gain_ref, gate_ref, up_ref, down_ref,
-        out_ref,
+        input_sem,
         local_ref, coef_ref, memory, lane_ref, plane_ref, mine_ref, carried_ref, mixed, gathered,
         matrix, stream_ref, rows_ref, hidden_ref, whole, own, inner, near, outer, far,
         relay_send, relay_recv, own_sem, lane_send, lane_recv, plane_send, plane_recv,
         load_sem, matrix_send, matrix_recv, out_sem, in_sem, row_send, row_recv,
         near_send, near_recv, far_send, far_recv,
-    ) = refs
+    ) = refs[25:]
     n = lay.n_tp
     rows, width = skip_ref.shape
     length, breadth = read_ref.shape
@@ -335,8 +364,6 @@
     for m in (GATE, UP):
         relay.forward(m, 0) if last else None
         relay.cross(m, 0)
-    for m in (GATE, UP, DOWN):
-        relay.own(m).start()
 
     def place_matrix(i, j):
         side, core = lax.rem(x + lay.sides - i, lay.sides), lax.rem(c + lay.cores - j, lay.cores)
@@ -353,6 +380,11 @@
             **to(tp=target),
         )
 
+    inputs = [
+        pltpu.make_async_copy(given[k], loaded[k], input_sem.at[k]) for k in range(len(given))
+    ]
+    for copy in inputs:
+        copy.start()
     own_matrix = pltpu.make_async_copy(matrix_ref, matrix.at[0, 0], load_sem)
     own_matrix.start()
     for i in range(1, lay.sides):
@@ -360,6 +392,8 @@
     for j in range(1, lay.cores):
         pass_matrix(0, j).start()
 
+    for m in (GATE, UP, DOWN):
+        relay.own(m).start()
     diagonal = jnp.where(
         lax.broadcasted_iota(jnp.int32, (PAIR, PAIR), 0)
         == lax.broadcasted_iota(jnp.int32, (PAIR, PAIR), 1),
@@ -371,21 +405,33 @@
         memory[p, PAIR:] = diagonal
 
     chunks = length // CHUNK
+    for copy in inputs[:6]:
+        copy.wait()
+
+    def gate_aside(first):
+        for lane in range(1, lay.lanes):
+            for hop, wanted in ((1, z > 0), (-1, z == 0)) if first else ((-1, z > 0),):
+                copy, held = relay.aside(GATE, hop, lane)
+                relay.start((copy, held & wanted))
 
     def one(turn, _):
         if last:
 
-            @pl.when(turn == chunks // 3)
+            @pl.when(turn == 5 * chunks // 12)
             def _():
                 relay.take(GATE, 1)
                 if last > 1:
                     relay.forward(GATE, 1)
-                for lane in range(1, lay.lanes):
-                    relay.start(relay.aside(GATE, 1, lane))
-
-            @pl.when(turn == 2 * chunks // 3)
+                gate_aside(True)
+
+            @pl.when(turn == 10 * chunks // 12)
             def _():
                 relay.take(UP, 1)
+                if last > 1:
+                    relay.forward(UP, 1)
+                for lane in range(1, lay.lanes):
+                    relay.arrive(UP, 0, lane)
+                relay.forward_wide(UP, 0)
 
         here = pl.ds(pl.multiple_of(turn * CHUNK, CHUNK), CHUNK)
         advance_chunk(
@@ -412,8 +458,7 @@
     for copy in lane_copies:
         copy.start()
     if last:
-        for lane in range(1, lay.lanes):
-            relay.start(relay.aside(GATE, -1, lane))
+        gate_aside(False)
         relay.cross(UP, 1)
     for copy in lane_copies:
         copy.wait_recv()
@@ -445,11 +490,13 @@
     for s in range(1, lay.planes):
         pl.when(z + s < lay.planes)(onward(s).start)
     if last > 1:
-        relay.forward(UP, 1)
-        relay.take(GATE, 2)
-        if last > 2:
-            relay.forward(GATE, 2)
-        relay.cross(GATE, 2)
+        for m in (GATE, UP):
+            relay.take(m, 2)
+            if last > 2:
+                relay.forward(m, 2)
+            relay.cross(m, 2)
+        relay.take_wide(UP, 1)
+        relay.forward_wide(UP, 1)
     for p in span:
         carried_ref[p] = jnp.zeros((PAIR, PAIR), f32)
     for s in range(last, 0, -1):
@@ -479,6 +526,7 @@
             **to(tp=peers[s]),
         )
 
+    inputs[6].wait()
     for s in range(n):
         target = peers[s] if s < n - 1 else me
         here = pl.ds(pl.multiple_of(target * rows, rows), rows)
@@ -501,14 +549,16 @@
                 gathered[s, :, at] = block
         if s < n - 1:
             send(s).start()
-    if last > 1:
-        relay.take(UP, 2)
-        if last > 2:
-            relay.forward(UP, 2)
-        relay.cross(UP, 2)
+    if last > 2:
+        relay.take_wide(UP, 2)
+        relay.forward_wide(UP, 2)
+        if last == 3:
+            relay.take(GATE, 3)
+            relay.cross(GATE, 3)
     for s in range(n - 1):
         send(s).wait_recv()
     own_matrix.wait()
+    inputs[7].wait()
     for i in range(lay.sides):
         for j in range(1, lay.cores):
             pass_matrix(i, j).wait_recv()
@@ -522,6 +572,9 @@
     scale = lax.rsqrt(jnp.mean(stream * stream, axis=-1, keepdims=True) + norm_eps)
     mine = pl.ds(pl.multiple_of(me * rows, rows), rows)
     rows_ref[mine] = (stream * scale * gain_ref[...]).astype(bf16)
+    if last:
+        relay.forward(DOWN, 0)
+    relay.cross(DOWN, 0)
 
     def pass_rows(source, target, slot):
         piece = rows_ref.at[pl.ds(pl.multiple_of(source * rows, rows), rows)]
@@ -548,13 +601,14 @@
             row_copies.append(copy)
     for r in range(3, last + 1):
         for m in (GATE, UP):
-            relay.take(m, r)
-            if r < last:
-                relay.forward(m, r)
-            relay.cross(m, r)
-    if last:
-        relay.forward(DOWN, 0)
-    relay.cross(DOWN, 0)
+            if m == UP or last > 3:
+                relay.take(m, r)
+                if r < last:
+                    relay.forward(m, r)
+                relay.cross(m, r)
+        if r < last:
+            relay.take_wide(UP, r)
+            relay.forward_wide(UP, r)
     for copy in row_copies[lay.sides - 1 :]:
         copy.wait_recv()
 
@@ -562,7 +616,10 @@
         relay.own(m).wait()
         for lane in range(1, lay.lanes):
             for hop in range(-last, last + 1):
-                relay.arrive(m, hop, lane)
+                if m in WIDE and hop == 0 and last:
+                    continue
+                taken = m in WIDE and 0 < abs(hop) < last
+                relay.arrive(m, hop, lane, wide=False if taken else None)
 
     def down_step(r):
         if r <= last:
@@ -571,7 +628,6 @@
                 relay.forward(DOWN, r)
             relay.cross(DOWN, r)
 
-    down_step(1)
     units = hidden_ref.shape[1]
     tile = 256 if units % 256 == 0 else 128 if units % 128 == 0 else units
     for first in range(0, units, tile):
@@ -610,7 +666,7 @@
 
     for t, hop in enumerate(hops):
         if hop >= 0:
-            down_step(hop + 2)
+            down_step(hop + 1)
         for lane in range(1, lay.lanes):
             relay.arrive(DOWN, hop, lane)
 
@@ -700,13 +756,19 @@
     hops = 2 * lay.planes - 1
     part = width // lay.planes
     dma = pltpu.SemaphoreType.DMA
+    given = (
+        acceptance_signal, lookup_mapped, payload_mapped, forget_dynamic_share,
+        additive_forget_logarithm, substitution_dynamic_share, result_switch, skip_stream,
+    )
     vmem, anywhere = pl.BlockSpec(memory_space=pltpu.VMEM), pl.BlockSpec(memory_space=pl.ANY)
     return pl.pallas_call(
         functools.partial(layer_kernel, lay, hops),
-        in_specs=[vmem] * 11 + [anywhere, vmem] + [anywhere] * 3,
+        in_specs=[vmem] * 4 + [anywhere] * 12,
         out_specs=vmem,
         out_shape=jax.ShapeDtypeStruct((rows, width), bf16),
-        scratch_shapes=[
+        scratch_shapes=[pltpu.VMEM(array.shape, array.dtype) for array in given]
+        + [
+            dma((len(given),)),
             pltpu.VMEM((length, breadth), f32),
             pltpu.VMEM((length, breadth), bf16),
             pltpu.VMEM((pairs, 2 * PAIR, PAIR), f32),
@@ -753,19 +815,12 @@
         ),
         name="layer",
     )(
-        skip_stream,
-        acceptance_signal,
-        lookup_mapped,
-        payload_mapped,
-        result_switch,
-        forget_dynamic_share,
-        additive_forget_logarithm,
         forget_feature_offset[None, :],
-        substitution_dynamic_share,
         substitution_feature_offset[None, :],
         diagonal_reward_scales[None, :],
+        mlp_rescaler[None, :],
+        *given,
         result_matrix,
-        mlp_rescaler[None, :],
         switch_matrix,
         expand_matrix,
         contract_matrix,

time: 212 us -> 184 us (0.87)
  Pallas kernels: 208 us -> 180 us
    pallas_call x1, Pallas kernels: 208 us -> 180 us  [per_device(): pl.pallas_call(functools.partial(layer_kernel, lay, hops), in_specs=[vmem...]
where the time goes in v2:
time: 184 us
  Pallas kernels  180 us (98%)
  local copies, waits for them, and re-layouts  3.74 us (2%)
    pallas_call x1, Pallas kernels, per_device(): pl.pallas_call(functools.partial(layer_kernel, lay, hops), in_specs=[vmem...  180 us
    unnamed x2, local copies, waits for them, and re-layouts  3.74 us

profile of v2, /device:TPU:0, one launch (start us, length us, event | category | flops | bytes accessed | tf_op | source)
XLA Modules:
  0.0 183.6 jit_solution(13452535816035059704)
XLA Ops:
  0.0 1.6 copy.17.refs_8_
  1.7 179.8 %layer.1 = bf16[192,2048]{1,0:T(8,128)(2,1)} custom-call(f32[1,512]{1,0:T(1,128)} %bitcast.5, f32[1,512]{1,0:T(1,128)} %bitcast.6, f32[1,512]{1,0:T(1,128)} %bitcast.7, f32[1,2048]{1,0:T(1,128)} %bitcast.4, bf16[768,512]{1,0:T(8,128)(2,1)} %refs_4_.1, bf16[768,512]{1,0:T(8,128)(2,1)} %refs_5_.1, bf16[768,512]{1,0:T(8,128)(2,1)} %refs_6_.1, ...), custom_call_target="tpu_custom_call" | custom-call | flops 12079595520 | bytes 15728640 | tf_op jit(solution)/shard_map/layer/pallas_call | solution.py:764
  181.5 2.1 %copy.19 = bf16[192,2048]{1,0:T(8,128)(2,1)} copy(bf16[192,2048]{1,0:T(8,128)(2,1)} %layer.1) | data formatting | bytes 1572864

commit v3 on v2

--- a/solution.py
+++ b/solution.py
@@ -211,8 +211,9 @@
     return mm(total, step, NN, 1) + mm(total - total.astype(bf16).astype(f32), step, NN, 1)
 
 
-GATE, UP, DOWN = range(3)
-WIDE = (UP,)
+GATE, UP, DOWN, LOW = range(4)
+WIDE = (UP, LOW)
+SHARE = {GATE: (0, 0, 1), UP: (1, 0, 1), DOWN: (2, 0, 2), LOW: (2, 1, 2)}
 
 
 class Relay:
@@ -239,12 +240,19 @@
         source = (self.z - hop) * self.lay.lanes + lax.rem(
             self.y + self.lay.lanes - lane, self.lay.lanes
         )
-        first = pl.multiple_of(source * self.depth, self.depth)
-        return self.whole.at[matrix, pl.ds(first, self.depth)]
+        array, share, shares = SHARE[matrix]
+        size = self.depth // shares
+        first = pl.multiple_of(source * self.depth + share * size, size)
+        return self.whole.at[array, pl.ds(first, size)]
+
+    def block(self, matrix):
+        array, share, shares = SHARE[matrix]
+        size = self.depth // shares
+        return self.blocks[array].at[pl.ds(share * size, size)]
 
     def copy(self, matrix, source, place, plane, lane):
         return pltpu.make_async_remote_copy(
-            src_ref=self.blocks[matrix] if source == (0, 0) else self.part(matrix, *source),
+            src_ref=self.block(matrix) if source == (0, 0) else self.part(matrix, *source),
             dst_ref=self.part(matrix, *source),
             send_sem=self.send_sem.at[matrix, self.slot(*place)],
             recv_sem=self.recv_sem.at[matrix, self.slot(*place)],
@@ -270,7 +278,7 @@
 
     def own(self, matrix):
         return pltpu.make_async_copy(
-            self.blocks[matrix], self.part(matrix, 0, 0), self.own_sem.at[matrix]
+            self.block(matrix), self.part(matrix, 0, 0), self.own_sem.at[matrix]
         )
 
     def arrive(self, matrix, hop, lane, wide=None):
@@ -330,9 +338,9 @@
     given, (matrix_ref, gate_ref, up_ref, down_ref) = given[:8], given[8:12]
     out_ref = refs[16]
     loaded = refs[17:25]
-    read_ref, key_ref, value_ref, forget_ref, added_ref, rate_ref, switch_ref, skip_ref = loaded
+    read_ref, key_ref, value_ref, forget_ref, heads_ref, rate_ref, switch_ref, skip_ref = loaded
     (
-        input_sem,
+        input_sem, added_ref,
         local_ref, coef_ref, memory, lane_ref, plane_ref, mine_ref, carried_ref, mixed, gathered,
         matrix, stream_ref, rows_ref, hidden_ref, whole, own, inner, near, outer, far,
         relay_send, relay_recv, own_sem, lane_send, lane_recv, plane_send, plane_recv,
@@ -392,7 +400,7 @@
     for j in range(1, lay.cores):
         pass_matrix(0, j).start()
 
-    for m in (GATE, UP, DOWN):
+    for m in SHARE:
         relay.own(m).start()
     diagonal = jnp.where(
         lax.broadcasted_iota(jnp.int32, (PAIR, PAIR), 0)
@@ -407,6 +415,7 @@
     chunks = length // CHUNK
     for copy in inputs[:6]:
         copy.wait()
+    added_ref[...] = heads_ref[...].T
 
     def gate_aside(first):
         for lane in range(1, lay.lanes):
@@ -432,6 +441,7 @@
                 for lane in range(1, lay.lanes):
                     relay.arrive(UP, 0, lane)
                 relay.forward_wide(UP, 0)
+                relay.cross(LOW, 0)
 
         here = pl.ds(pl.multiple_of(turn * CHUNK, CHUNK), CHUNK)
         advance_chunk(
@@ -474,21 +484,22 @@
             if t < lay.lanes - 1:
                 own_state[p] = jnp.where(y > t, state[p], own_state[p])
                 own_move[p] = jnp.where(y > t, move[p], own_move[p])
-    for p in span:
-        mine_ref[0, p] = fold(state[p]).astype(bf16)
-        mine_ref[1, p] = fold(move[p]).astype(bf16)
-
-    def onward(s):
-        return pltpu.make_async_remote_copy(
-            src_ref=mine_ref,
-            dst_ref=plane_ref.at[s - 1],
-            send_sem=plane_send.at[s - 1],
-            recv_sem=plane_recv.at[s - 1],
-            **to(sp=line[s - 1]),
-        )
-
-    for s in range(1, lay.planes):
-        pl.when(z + s < lay.planes)(onward(s).start)
+    onward = pltpu.make_async_remote_copy(
+        src_ref=mine_ref,
+        dst_ref=plane_ref,
+        send_sem=plane_send,
+        recv_sem=plane_recv,
+        **to(sp=lax.rem(spot + lay.lanes, lay.n_sp)),
+    )
+
+    def pass_on(carried):
+        for p in span:
+            total = state[p] if carried is None else chain(carried[p], move[p]) + state[p]
+            mine_ref[p] = fold(total).astype(bf16)
+        onward.start()
+
+    if last:
+        pl.when(z == 0)(functools.partial(pass_on, None))
     if last > 1:
         for m in (GATE, UP):
             relay.take(m, 2)
@@ -498,19 +509,20 @@
         relay.take_wide(UP, 1)
         relay.forward_wide(UP, 1)
     for p in span:
-        carried_ref[p] = jnp.zeros((PAIR, PAIR), f32)
-    for s in range(last, 0, -1):
-
-        @pl.when(z >= s)
-        def _(s=s):
-            onward(s).wait_recv()
+        carried_ref[p] = own_state[p]
+    if last:
+
+        @pl.when(z > 0)
+        def _():
+            onward.wait_recv()
+            carried = [stack(plane_ref[p].astype(f32)) for p in span]
+
+            @pl.when(z < last)
+            def _():
+                pass_on(carried)
+
             for p in span:
-                carried_ref[p] = chain(
-                    carried_ref[p], stack(plane_ref[s - 1, 1, p].astype(f32))
-                ) + stack(plane_ref[s - 1, 0, p].astype(f32))
-
-    for p in span:
-        carried_ref[p] = chain(carried_ref[p], own_move[p]) + own_state[p]
+                carried_ref[p] = chain(carried[p], own_move[p]) + own_state[p]
 
     for i in range(1, lay.sides):
         pass_matrix(i, 0).wait_recv()
@@ -574,7 +586,14 @@
     rows_ref[mine] = (stream * scale * gain_ref[...]).astype(bf16)
     if last:
         relay.forward(DOWN, 0)
+        relay.forward(LOW, 0)
     relay.cross(DOWN, 0)
+    if last:
+        for lane in range(1, lay.lanes):
+            relay.arrive(LOW, 0, lane)
+        relay.forward_wide(LOW, 0)
+    else:
+        relay.cross(LOW, 0)
 
     def pass_rows(source, target, slot):
         piece = rows_ref.at[pl.ds(pl.multiple_of(source * rows, rows), rows)]
@@ -622,11 +641,16 @@
                 relay.arrive(m, hop, lane, wide=False if taken else None)
 
     def down_step(r):
-        if r <= last:
-            relay.take(DOWN, r)
+        if r > last:
+            return
+        if r > 1:
+            relay.take_wide(LOW, r - 1)
+            relay.forward_wide(LOW, r - 1)
+        for m in (DOWN, LOW):
+            relay.take(m, r)
             if r < last:
-                relay.forward(DOWN, r)
-            relay.cross(DOWN, r)
+                relay.forward(m, r)
+            relay.cross(m, r)
 
     units = hidden_ref.shape[1]
     tile = 256 if units % 256 == 0 else 128 if units % 128 == 0 else units
@@ -637,6 +661,7 @@
         hidden_ref[:, columns] = (gated * jax.nn.sigmoid(gated) * raised).astype(bf16)
 
     relay.own(DOWN).wait()
+    relay.own(LOW).wait()
     part = width // lay.planes
     order = list(range(1, lay.sides)) + [0]
     hops = [0] + [way * r for r in range(1, last + 1) for way in (1, -1)]
@@ -669,6 +694,9 @@
             down_step(hop + 1)
         for lane in range(1, lay.lanes):
             relay.arrive(DOWN, hop, lane)
+            if hop or not last:
+                taken = 0 < abs(hop) < last
+                relay.arrive(LOW, hop, lane, wide=False if taken else None)
 
         @pl.when(relay.held(hop))
         def _(t=t, hop=hop):
@@ -702,12 +730,12 @@
             sums = sums.astype(bf16).astype(f32)
             out_ref[:, columns] = (stream_ref[:, columns] + half_step * sums).astype(bf16)
 
-    for m in (GATE, UP, DOWN):
+    for m in SHARE:
         relay.settle(m)
     for copy in lane_copies + row_copies:
         copy.wait_send()
-    for s in range(1, lay.planes):
-        pl.when(z + s < lay.planes)(onward(s).wait_send)
+    if last:
+        pl.when(z < last)(onward.wait_send)
     for i in range(lay.sides):
         for j in range(lay.cores):
             if i or j:
@@ -750,7 +778,7 @@
     pairs = breadth // PAIR
     n = lay.n_tp
     one = (2, pairs, PER_GROUP_DIMS, PAIR)
-    lanes, planes = max(lay.lanes - 1, 1), max(lay.planes - 1, 1)
+    lanes = max(lay.lanes - 1, 1)
     cores, sides = max(lay.cores - 1, 1), max(lay.sides - 1, 1)
     places = (2 * lay.planes - 1) * lay.lanes
     hops = 2 * lay.planes - 1
@@ -758,7 +786,7 @@
     dma = pltpu.SemaphoreType.DMA
     given = (
         acceptance_signal, lookup_mapped, payload_mapped, forget_dynamic_share,
-        additive_forget_logarithm, substitution_dynamic_share, result_switch, skip_stream,
+        additive_forget_logarithm.T, substitution_dynamic_share, result_switch, skip_stream,
     )
     vmem, anywhere = pl.BlockSpec(memory_space=pltpu.VMEM), pl.BlockSpec(memory_space=pl.ANY)
     return pl.pallas_call(
@@ -769,12 +797,13 @@
         scratch_shapes=[pltpu.VMEM(array.shape, array.dtype) for array in given]
         + [
             dma((len(given),)),
+            pltpu.VMEM(additive_forget_logarithm.shape, f32),
             pltpu.VMEM((length, breadth), f32),
             pltpu.VMEM((length, breadth), bf16),
             pltpu.VMEM((pairs, 2 * PAIR, PAIR), f32),
             pltpu.VMEM((lay.lanes,) + one, bf16),
-            pltpu.VMEM((planes,) + one, bf16),
-            pltpu.VMEM(one, bf16),
+            pltpu.VMEM(one[1:], bf16),
+            pltpu.VMEM(one[1:], bf16),
             pltpu.VMEM((pairs, PAIR, PAIR), f32),
             pltpu.VMEM((n - 1, rows, breadth), bf16),
             pltpu.VMEM((n, rows, breadth), bf16),
@@ -788,13 +817,13 @@
             pltpu.VMEM((hops, cores, lay.sides, rows, part), bf16),
             pltpu.VMEM((hops, sides, rows, part), bf16),
             pltpu.VMEM((hops, sides, rows, part), bf16),
-            dma((3, places)),
-            dma((3, places)),
-            dma((3,)),
+            dma((len(SHARE), places)),
+            dma((len(SHARE), places)),
+            dma((len(SHARE),)),
             dma((lanes,)),
             dma((lanes,)),
-            dma((planes,)),
-            dma((planes,)),
+            dma,
+            dma,
             dma,
             dma((lay.sides, lay.cores)),
             dma((lay.sides, lay.cores)),

time: 184 us -> 180 us (0.978)
  the two profiles are of different devices: /device:TPU:0 before, /device:TPU:24 now
where the time goes in v3:
time: 180 us
  Pallas kernels  178 us (99%)
  local copies, waits for them, and re-layouts  2.09 us (1%)
    pallas_call x1, Pallas kernels, per_device(): pl.pallas_call(functools.partial(layer_kernel, lay, hops), in_specs=[vmem...  178 us

profile of v3, /device:TPU:24, one launch (start us, length us, event | category | flops | bytes accessed | tf_op | source)
XLA Modules:
  0.0 180.3 jit_solution(17857965031150185357)
XLA Ops:
  0.0 178.2 %layer.1 = bf16[192,2048]{1,0:T(8,128)(2,1)} custom-call(f32[1,512]{1,0:T(1,128)} %bitcast.7, f32[1,512]{1,0:T(1,128)} %bitcast.8, f32[1,512]{1,0:T(1,128)} %bitcast.9, f32[1,2048]{1,0:T(1,128)} %bitcast.6, bf16[768,512]{1,0:T(8,128)(2,1)} %refs_4_.1, bf16[768,512]{1,0:T(8,128)(2,1)} %refs_5_.1, bf16[768,512]{1,0:T(8,128)(2,1)} %refs_6_.1, ...), custom_call_target="tpu_custom_call" | custom-call | flops 12079595520 | bytes 15728640 | tf_op jit(solution)/shard_map/layer/pallas_call | solution.py:792
  178.2 2.1 %copy.18 = bf16[192,2048]{1,0:T(8,128)(2,1)} copy(bf16[192,2048]{1,0:T(8,128)(2,1)} %layer.1) | data formatting | bytes 1572864
